TPU v7x, 32 devices: a whole 2x2x4 slice. The times are simulated.
32 devices in a mesh: tp: 8 (over z, y), dp: 4 (over x, core).
Axes of the slice: x: 2, y: 2, z: 4, core: 2. Of those that a mesh axis runs over, the one named last changes fastest.
Arguments:
- stream: bfloat16 [256, 2048], P('tp', 'dp'), may hold values from -12 to 12
- norm_gain: float32 [2, 2048], P(None, 'dp'), may hold values from 0.1 to 1.9
- w_input: bfloat16 [2, 2048, 2048], P(None, 'dp', 'tp'), may hold values from -0.125 to 0.125
- lam_re: float32 [2, 128, 64], P(None, 'tp'), may hold values from -1 to -0.05
- lam_im: float32 [2, 128, 64], P(None, 'tp'), may hold values from 0 to 6
- log_dt: float32 [2, 128], P(None, 'tp'), may hold values from -3 to 0
- b_re: float32 [2, 128, 64, 16], P(None, 'tp'), may hold values from -1 to 1
- b_im: float32 [2, 128, 64, 16], P(None, 'tp'), may hold values from -1 to 1
- readout_real: float32 [2, 128, 16, 64], P(None, 'tp'), may hold values from -0.5 to 0.5
- readout_imaginary: float32 [2, 128, 16, 64], P(None, 'tp'), may hold values from -0.5 to 0.5
- d_skip: float32 [2, 2048], P(None, 'tp'), may hold values from -4 to 4
- w_val: bfloat16 [2, 2048, 2048], P(None, 'tp', 'dp'), may hold values from -0.375 to 0.375
- w_gate: bfloat16 [2, 2048, 2048], P(None, 'tp', 'dp'), may hold values from -0.375 to 0.375
- state: float32 [2, 256, 128, 128], P(None, 'dp', 'tp'), may hold values from -6 to 6
Outputs:
- stream_out: bfloat16 [256, 2048], P('tp', 'dp')
- states_out: float32 [2, 256, 128, 128], P(None, 'dp', 'tp')
All inputs are finite; a program needn't handle non-finite values.
Results may differ from a plain program's by a relative error of at most 0.0064.
Values may be sent and summed in bfloat16 or wider, within the bound.
A program may use at most 64 MiB of HBM per device.

v0:
```python
import jax
import jax.numpy as jnp
from jax import lax
from jax.sharding import PartitionSpec as P

D = 2048
LAYERS = 2
eps = 1e-06


def advance(
    inputs, old_state, lam_re, lam_im, log_dt, b_re, b_im, readout_real, readout_imaginary, d_skip
):
    upper_bound = lax.Precision.HIGHEST
    count_rows, groups, doubled = old_state.shape
    half_state = doubled // 2
    chans = b_re.shape[-1]
    step_size = jnp.exp(log_dt)[:, None]
    decay = jnp.exp(lam_re * step_size)
    angle = lam_im * step_size
    keep_re = decay * jnp.cos(angle)
    keep_im = decay * jnp.sin(angle)
    denom = lam_re * lam_re + lam_im * lam_im
    ratio_re = ((keep_re - 1.0) * lam_re + keep_im * lam_im) / denom
    ratio_im = (keep_im * lam_re - (keep_re - 1.0) * lam_im) / denom
    drive_re = ratio_re[..., None] * b_re - ratio_im[..., None] * b_im
    drive_im = ratio_re[..., None] * b_im + ratio_im[..., None] * b_re
    grouped = inputs.reshape(count_rows, groups, chans)
    push_re = jnp.einsum("gpc,rgc->rgp", drive_re, grouped, precision=upper_bound)
    push_im = jnp.einsum("gpc,rgc->rgp", drive_im, grouped, precision=upper_bound)
    old_re = old_state[..., :half_state]
    old_im = old_state[..., half_state:]
    updated_real = keep_re * old_re - keep_im * old_im + push_re
    updated_imaginary = keep_re * old_im + keep_im * old_re + push_im
    readout_output = jnp.einsum(
        "aot,mat->mao", readout_real, updated_real, precision=upper_bound
    ) - jnp.einsum("aot,mat->mao", readout_imaginary, updated_imaginary, precision=upper_bound)
    pre_act = readout_output.reshape(count_rows, groups * chans) + d_skip * inputs
    return (pre_act, jnp.concatenate([updated_real, updated_imaginary], axis=-1))


def half_output(mixed_all, val_part, gate_part):
    return jnp.concatenate(
        [
            jnp.dot(mixed_all, val_part, preferred_element_type=jnp.float32),
            jnp.dot(mixed_all, gate_part, preferred_element_type=jnp.float32),
        ],
        axis=1,
    )


def per_device(
    stream,
    norm_gain,
    w_input,
    lam_re,
    lam_im,
    log_dt,
    b_re,
    b_im,
    readout_real,
    readout_imaginary,
    d_skip,
    w_val,
    w_gate,
    state,
):
    collected = []
    for layer_no in range(LAYERS):
        gathered = lax.all_gather(stream, "tp", axis=0, tiled=True)
        widened = gathered.astype(jnp.float32)
        normed = (widened * norm_gain[layer_no]).astype(jnp.bfloat16)
        square_part = jnp.sum(widened * widened, axis=1)
        weight_in = w_input[layer_no]
        partial_value = jnp.dot(normed, weight_in, preferred_element_type=jnp.float32)
        summed, square_total = (
            lax.psum_scatter(partial_value, "dp", scatter_dimension=0, tiled=True),
            lax.psum_scatter(square_part, "dp", scatter_dimension=0, tiled=True),
        )
        inputs = lax.rsqrt(square_total / D + eps)[:, None] * summed
        pre_act, new_state = advance(
            inputs,
            state[layer_no],
            lam_re[layer_no],
            lam_im[layer_no],
            log_dt[layer_no],
            b_re[layer_no],
            b_im[layer_no],
            readout_real[layer_no],
            readout_imaginary[layer_no],
            d_skip[layer_no],
        )
        mixed = jax.nn.gelu(pre_act).astype(jnp.bfloat16)
        mixed_all = lax.all_gather(mixed, "dp", axis=0, tiled=True)
        columns = w_val.shape[2]
        combined = lax.psum_scatter(
            half_output(mixed_all, w_val[layer_no], w_gate[layer_no]),
            "tp",
            scatter_dimension=0,
            tiled=True,
        )
        value = combined[:, :columns]
        gate = combined[:, columns:]
        stream = (stream.astype(jnp.float32) + value * jax.nn.sigmoid(gate)).astype(jnp.bfloat16)
        collected.append(new_state)
    return (stream, jnp.stack(collected))


def solution(mesh):
    return jax.shard_map(
        per_device,
        mesh=mesh,
        in_specs=(
            P("tp", "dp"),
            P(None, "dp"),
            P(None, "dp", "tp"),
            P(None, "tp", None),
            P(None, "tp", None),
            P(None, "tp"),
            P(None, "tp", None, None),
            P(None, "tp", None, None),
            P(None, "tp", None, None),
            P(None, "tp", None, None),
            P(None, "tp"),
            P(None, "tp", "dp"),
            P(None, "tp", "dp"),
            P(None, "dp", "tp", None),
        ),
        out_specs=(P("tp", "dp"), P(None, "dp", "tp", None)),
        check_vma=False,
    )
```

profile of v0, /device:TPU:0, one launch (start us, length us, event | category | flops | bytes accessed | tf_op | source)
XLA Modules:
  0.0 278.8 jit_solution(17151186009216203104)
XLA Ops:
  7.2 0.8 fusion.109
  8.0 32.8 %all_gather.12 = bf16[256,512]{1,0:T(8,128)(2,1)S(1)} all-gather(bf16[32,512]{1,0:T(8,128)(2,1)} %param.14), channel_id=1, replica_groups=mesh['tp'=8,'dp'=4] {'tp'}, dimensions={0}, use_global_device_ids=true | all-gather | bytes 294912 | tf_op jit(solution)/shard_map/all_gather | solution.py:70
  40.8 1.9 fusion.10
  42.8 0.7 copy-done.18
  44.4 5.6 %all-reduce = f32[256]{0:T(256)S(1)} all-reduce(f32[256]{0:T(256)S(1)} %fusion.4), channel_id=2, replica_groups=mesh['tp'=8,'dp'=4] {'dp'}, use_global_device_ids=true, to_apply=%region_1.0.clone | all-reduce | flops 256 | bytes 2048
  50.1 0.7 copy-done.19
  52.5 11.4 %reduce-scatter.5.cloned.1.call-done = f32[64,256]{1,0:T(8,128)} async-done(((f32[256,256]{1,0:T(8,128)}), f32[64,256]{1,0:T(8,128)}) %reduce-scatter.5.cloned.1.call-update) | async-done | bytes 65552 | tf_op jit(solution)/shard_map/reduce_scatter | solution.py:77
  63.9 0.9 broadcast_multiply_fusion.1
  64.9 1.0 fusion.3
  65.9 1.0 fusion.2
  67.0 0.9 fusion.38
  68.0 0.9 convolution_subtract_fusion.1
  69.0 0.8 copy-done.10
  69.8 5.5 %all_gather.13 = bf16[256,256]{1,0:T(8,128)(2,1)S(1)} all-gather(bf16[64,256]{1,0:T(8,128)(2,1)S(1)} %fusion.63), channel_id=1, replica_groups=mesh['tp'=8,'dp'=4] {'dp'}, dimensions={0}, use_global_device_ids=true | all-gather | bytes 163840 | tf_op jit(solution)/shard_map/all_gather | solution.py:94
  75.9 1.1 pad_maximum_fusion
  77.0 64.3 %reduce-scatter.7.cloned.1.call-done = f32[32,1024]{1,0:T(8,128)} async-done(((f32[256,1024]{1,0:T(8,128)}), f32[32,1024]{1,0:T(8,128)}) %reduce-scatter.7.cloned.1.call-update) | async-done | bytes 131088 | tf_op jit(solution)/shard_map/reduce_scatter | solution.py:96
  141.4 0.9 fusion.90
  142.3 30.9 %all_gather.14 = bf16[256,512]{1,0:T(8,128)(2,1)S(1)} all-gather(bf16[32,512]{1,0:T(8,128)(2,1)S(1)} %fusion.90), channel_id=1, replica_groups=mesh['tp'=8,'dp'=4] {'tp'}, dimensions={0}, use_global_device_ids=true | all-gather | bytes 294912 | tf_op jit(solution)/shard_map/all_gather | solution.py:70
  173.1 0.9 fusion.8
  174.3 5.7 %all-reduce.1 = f32[256]{0:T(256)S(1)} all-reduce(f32[256]{0:T(256)S(1)} %fusion.6), channel_id=5, replica_groups=mesh['tp'=8,'dp'=4] {'dp'}, use_global_device_ids=true, to_apply=%region_5.0.clone | all-reduce | flops 256 | bytes 2048
  180.0 13.2 %reduce-scatter.9.cloned.1.call-done = f32[64,256]{1,0:T(8,128)} async-done(((f32[256,256]{1,0:T(8,128)}), f32[64,256]{1,0:T(8,128)}) %reduce-scatter.9.cloned.1.call-update) | async-done | bytes 65552 | tf_op jit(solution)/shard_map/reduce_scatter | solution.py:77
  193.2 0.9 broadcast_multiply_fusion
  194.3 1.0 fusion
  195.3 1.0 fusion.1
  196.4 0.9 fusion.31
  197.3 0.9 convolution_subtract_fusion
  198.4 0.8 copy-done.11
  199.2 5.5 %all_gather.15 = bf16[256,256]{1,0:T(8,128)(2,1)S(1)} all-gather(bf16[64,256]{1,0:T(8,128)(2,1)S(1)} %fusion.71), channel_id=1, replica_groups=mesh['tp'=8,'dp'=4] {'dp'}, dimensions={0}, use_global_device_ids=true | all-gather | bytes 163840 | tf_op jit(solution)/shard_map/all_gather | solution.py:94
  205.2 1.1 pad_maximum_fusion.1
  206.9 1.6 copy.38
  208.5 62.3 %reduce-scatter.11.cloned.1.call-done = f32[32,1024]{1,0:T(8,128)} async-done(((f32[256,1024]{1,0:T(8,128)}), f32[32,1024]{1,0:T(8,128)}) %reduce-scatter.11.cloned.1.call-update) | async-done | bytes 131088 | tf_op jit(solution)/shard_map/reduce_scatter | solution.py:96
  270.7 1.5 fusion.91
  (68 shorter events, 4.5 us)
Async XLA Ops:
  7.2 44.9 %copy-start.2 = (f32[2,64,16,128]{3,2,1,0:T(8,128)S(1)}, f32[2,64,16,128]{3,2,1,0:T(8,128)}, u32[]{:S(2)}) copy-start(f32[2,64,16,128]{3,2,1,0:T(8,128)} %param.27) | copy-start | bytes 3145732
  7.2 56.7 %reduce-scatter.5.cloned.1.call-start = ((), (), s32[]{:S(2)}) async-start(), calls=%async_computation.4 | async-start | bytes 327680 | tf_op jit(solution)/shard_map/reduce_scatter | solution.py:77
  42.7 0.8 copy-start.15
  42.7 0.8 copy-start.16
  42.7 98.7 %reduce-scatter.7.cloned.1.call-start = ((), (), s32[]{:S(2)}) async-start(), calls=%async_computation.5 | async-start | bytes 1179648 | tf_op jit(solution)/shard_map/reduce_scatter | solution.py:96
  42.7 0.7 copy-start.18
  43.7 0.7 copy-start.17
  50.1 0.7 copy-start.19
  52.1 12.7 %copy-start.1 = (f32[2,16,64,16]{2,3,1,0:T(8,128)S(1)}, f32[2,16,64,16]{2,3,1,0:T(8,128)}, u32[]{:S(2)}) copy-start(f32[2,16,64,16]{2,3,1,0:T(8,128)} %param.20) | copy-start | bytes 393220
  52.5 12.4 %copy-start = (f32[2,16,64,16]{2,3,1,0:T(8,128)S(1)}, f32[2,16,64,16]{2,3,1,0:T(8,128)}, u32[]{:S(2)}) copy-start(f32[2,16,64,16]{2,3,1,0:T(8,128)} %param.21) | copy-start | bytes 393220
  65.9 1.1 copy-start.12
  67.0 1.0 copy-start.8
  68.0 7.5 %copy-start.4 = (bf16[2,256,512]{2,1,0:T(8,128)(2,1)S(1)}, bf16[2,256,512]{2,1,0:T(8,128)(2,1)}, u32[]{:S(2)}) copy-start(bf16[2,256,512]{2,1,0:T(8,128)(2,1)} %param.26) | copy-start | bytes 1572868
  68.9 0.9 copy-start.10
  69.8 5.8 %copy-start.6 = (bf16[2,256,512]{2,1,0:T(8,128)(2,1)S(1)}, bf16[2,256,512]{2,1,0:T(8,128)(2,1)}, u32[]{:S(2)}) copy-start(bf16[2,256,512]{2,1,0:T(8,128)(2,1)} %param.25) | copy-start | bytes 1572868
  76.9 64.4 %copy-start.14 = (bf16[32,512]{1,0:T(8,128)(2,1)S(1)}, bf16[32,512]{1,0:T(8,128)(2,1)}, u32[]{:S(2)}) copy-start(bf16[32,512]{1,0:T(8,128)(2,1)} %param.14) | copy-start | bytes 98308
  76.9 96.2 %copy-start.3 = (bf16[2,512,256]{2,1,0:T(8,128)(2,1)S(1)}, bf16[2,512,256]{2,1,0:T(8,128)(2,1)}, u32[]{:S(2)}) copy-start(bf16[2,512,256]{2,1,0:T(8,128)(2,1)} %param.16) | copy-start | bytes 1572868
  77.0 116.3 %reduce-scatter.9.cloned.1.call-start = ((), (), s32[]{:S(2)}) async-start(), calls=%async_computation.6 | async-start | bytes 327680 | tf_op jit(solution)/shard_map/reduce_scatter | solution.py:77
  174.1 96.6 %reduce-scatter.11.cloned.1.call-start = ((), (), s32[]{:S(2)}) async-start(), calls=%async_computation.7 | async-start | bytes 1179648 | tf_op jit(solution)/shard_map/reduce_scatter | solution.py:96
  195.3 1.1 copy-start.13
  196.4 1.0 copy-start.9
  197.3 7.4 %copy-start.5 = (bf16[2,256,512]{2,1,0:T(8,128)(2,1)S(1)}, bf16[2,256,512]{2,1,0:T(8,128)(2,1)}, u32[]{:S(2)}) copy-start(bf16[2,256,512]{2,1,0:T(8,128)(2,1)} %param.26) | copy-start | bytes 1572868
  198.3 0.9 copy-start.11
  199.2 5.8 %copy-start.7 = (bf16[2,256,512]{2,1,0:T(8,128)(2,1)S(1)}, bf16[2,256,512]{2,1,0:T(8,128)(2,1)}, u32[]{:S(2)}) copy-start(bf16[2,256,512]{2,1,0:T(8,128)(2,1)} %param.25) | copy-start | bytes 1572868
Sparse Core Ops, SparseCore 0:
  42.8 21.0 reduce-scatter.4
  77.1 64.2 reduce-scatter.6
  174.2 18.9 reduce-scatter.8
  206.5 64.2 reduce-scatter.10
where the time goes:
time: 279 us
  waiting for transfers between devices  151 us (54%)
  blocking collectives  86 us (31%)
  between operations  14.7 us (5%)
  matrix products  11.6 us (4%)
  other arithmetic  7.83 us (3%)
  local copies, waits for them, and re-layouts  7.2 us (3%)
    reduce_scatter x2, waiting for transfers between devices, per_device(): lax.psum_scatter(half_output(mixed_all, w_val[layer_no], w_gate[layer_no]...  127 us
    all_gather x2, blocking collectives, per_device(): gathered = lax.all_gather(stream, 'tp', axis=0, tiled=True)  63.6 us
    reduce_scatter x2, waiting for transfers between devices, per_device(): lax.psum_scatter(partial_value, 'dp', scatter_dimension=0, tiled=True)  24.6 us
    unnamed x2, blocking collectives  11.3 us
    all_gather x2, blocking collectives, per_device(): mixed_all = lax.all_gather(mixed, 'dp', axis=0, tiled=True)  11.1 us
    unnamed x42, local copies, waits for them, and re-layouts  5.66 us
  transfers between devices with their start and end apart: 4, of which 4 were waited for; matrix products, arithmetic and copies ran while one was open for 1% of the time, Pallas kernels for 0%

commit v1 on v0

--- a/solution.py
+++ b/solution.py
@@ -67,7 +67,14 @@
 ):
     collected = []
     for layer_no in range(LAYERS):
-        gathered = lax.all_gather(stream, "tp", axis=0, tiled=True)
+        ring = [stream]
+        for hop in range(7):
+            ring.append(lax.ppermute(ring[-1], "tp", [(dev, (dev + 1) % 8) for dev in range(8)]))
+        gathered = jnp.roll(
+            jnp.concatenate(ring[::-1], axis=0),
+            (lax.axis_index("tp") + 1) * ring[0].shape[0],
+            axis=0,
+        )
         widened = gathered.astype(jnp.float32)
         normed = (widened * norm_gain[layer_no]).astype(jnp.bfloat16)
         square_part = jnp.sum(widened * widened, axis=1)

time: 279 us -> 305 us (1.093)
  waiting for transfers between devices: 151 us -> 235 us
  blocking collectives: 86 us -> 22.4 us
  starting transfers between devices: 0.16 us -> 4.35 us
    ppermute x0 -> x14, waiting for transfers between devices: none -> 88.7 us  [per_device(): lax.ppermute(ring[-1], 'tp', [(dev, (dev + 1) % 8) for dev in range(8)])]
    all_gather x2 -> x0, blocking collectives: 63.6 us -> none  [per_device(): gathered = lax.all_gather(stream, 'tp', axis=0, tiled=True)]
    reduce_scatter x2, waiting for transfers between devices: 24.6 us -> 19.8 us  [per_device(): lax.psum_scatter(partial_value, 'dp', scatter_dimension=0, tiled=True)]
    ppermute x0 -> x14, starting transfers between devices: none -> 4.19 us  [per_device(): lax.ppermute(ring[-1], 'tp', [(dev, (dev + 1) % 8) for dev in range(8)])]
  transfers between devices with their start and end apart: 4 -> 18, of which waited for: 4 -> 18; matrix products, arithmetic and copies ran while one was open for 1% -> 2% of each run, Pallas kernels for 0% -> 0%
where the time goes in v1:
time: 305 us
  waiting for transfers between devices  235 us (77%)
  blocking collectives  22.4 us (7%)
  between operations  14.8 us (5%)
  matrix products  11.8 us (4%)
  other arithmetic  8.2 us (3%)
  local copies, waits for them, and re-layouts  7.87 us (3%)
  starting transfers between devices  4.35 us (1%)
    reduce_scatter x2, waiting for transfers between devices, per_device(): lax.psum_scatter(half_output(mixed_all, w_val[layer_no], w_gate[layer_no]...  127 us
    ppermute x14, waiting for transfers between devices, per_device(): lax.ppermute(ring[-1], 'tp', [(dev, (dev + 1) % 8) for dev in range(8)])  88.7 us
    reduce_scatter x2, waiting for transfers between devices, per_device(): lax.psum_scatter(partial_value, 'dp', scatter_dimension=0, tiled=True)  19.8 us
    unnamed x2, blocking collectives  11.3 us
    all_gather x2, blocking collectives, per_device(): mixed_all = lax.all_gather(mixed, 'dp', axis=0, tiled=True)  11.1 us
  transfers between devices with their start and end apart: 18, of which 18 were waited for; matrix products, arithmetic and copies ran while one was open for 2% of the time, Pallas kernels for 0%

profile of v1, /device:TPU:0, one launch (start us, length us, event | category | flops | bytes accessed | tf_op | source)
XLA Modules:
  0.0 304.8 jit_solution(7720905931886888201)
XLA Ops:
  7.2 3.0 collective-permute-start
  10.3 5.1 %collective-permute-done = bf16[32,512]{1,0:T(8,128)(2,1)S(1)} collective-permute-done((bf16[32,512]{1,0:T(8,128)(2,1)}, bf16[32,512]{1,0:T(8,128)(2,1)S(1)}, u32[]{:S(2)}, u32[]{:S(2)}) %collective-permute-start) | collective-permute-done | bytes 32800 | tf_op jit(solution)/shard_map/ppermute | solution.py:72
  15.4 6.6 %collective-permute-done.1 = bf16[32,512]{1,0:T(8,128)(2,1)S(1)} collective-permute-done((bf16[32,512]{1,0:T(8,128)(2,1)S(1)}, bf16[32,512]{1,0:T(8,128)(2,1)S(1)}, u32[]{:S(2)}, u32[]{:S(2)}) %collective-permute-start.1) | collective-permute-done | bytes 32800 | tf_op jit(solution)/shard_map/ppermute | solution.py:72
  22.0 1.3 fusion.112
  23.4 5.3 %collective-permute-done.2 = bf16[32,512]{1,0:T(8,128)(2,1)S(1)} collective-permute-done((bf16[32,512]{1,0:T(8,128)(2,1)S(1)}, bf16[32,512]{1,0:T(8,128)(2,1)S(1)}, u32[]{:S(2)}, u32[]{:S(2)}) %collective-permute-start.2) | collective-permute-done | bytes 32800 | tf_op jit(solution)/shard_map/ppermute | solution.py:72
  28.7 6.6 %collective-permute-done.3 = bf16[32,512]{1,0:T(8,128)(2,1)S(1)} collective-permute-done((bf16[32,512]{1,0:T(8,128)(2,1)S(1)}, bf16[32,512]{1,0:T(8,128)(2,1)S(1)}, u32[]{:S(2)}, u32[]{:S(2)}) %collective-permute-start.3) | collective-permute-done | bytes 32800 | tf_op jit(solution)/shard_map/ppermute | solution.py:72
  35.4 6.8 %collective-permute-done.4 = bf16[32,512]{1,0:T(8,128)(2,1)S(1)} collective-permute-done((bf16[32,512]{1,0:T(8,128)(2,1)S(1)}, bf16[32,512]{1,0:T(8,128)(2,1)S(1)}, u32[]{:S(2)}, u32[]{:S(2)}) %collective-permute-start.4) | collective-permute-done | bytes 32800 | tf_op jit(solution)/shard_map/ppermute | solution.py:72
  42.4 6.5 %collective-permute-done.5 = bf16[32,512]{1,0:T(8,128)(2,1)S(1)} collective-permute-done((bf16[32,512]{1,0:T(8,128)(2,1)S(1)}, bf16[32,512]{1,0:T(8,128)(2,1)S(1)}, u32[]{:S(2)}, u32[]{:S(2)}) %collective-permute-start.5) | collective-permute-done | bytes 32800 | tf_op jit(solution)/shard_map/ppermute | solution.py:72
  48.8 6.6 %collective-permute-done.6 = bf16[32,512]{1,0:T(8,128)(2,1)S(1)} collective-permute-done((bf16[32,512]{1,0:T(8,128)(2,1)S(1)}, bf16[32,512]{1,0:T(8,128)(2,1)S(1)}, u32[]{:S(2)}, u32[]{:S(2)}) %collective-permute-start.6) | collective-permute-done | bytes 32800 | tf_op jit(solution)/shard_map/ppermute | solution.py:72
  56.2 1.1 fusion.12
  60.6 5.7 %all-reduce = f32[256]{0:T(256)S(1)} all-reduce(f32[256]{0:T(256)S(1)} %fusion.4), channel_id=2, replica_groups=mesh['tp'=8,'dp'=4] {'dp'}, use_global_device_ids=true, to_apply=%region_1.3.clone | all-reduce | flops 256 | bytes 2048
  66.3 8.5 %reduce-scatter.5.cloned.1.call-done = f32[64,256]{1,0:T(8,128)} async-done(((f32[256,256]{1,0:T(8,128)}), f32[64,256]{1,0:T(8,128)}) %reduce-scatter.5.cloned.1.call-update) | async-done | bytes 65552 | tf_op jit(solution)/shard_map/reduce_scatter | solution.py:84
  80.8 5.5 %all_gather.6 = bf16[256,256]{1,0:T(8,128)(2,1)S(1)} all-gather(bf16[64,256]{1,0:T(8,128)(2,1)S(1)} %fusion.65), channel_id=1, replica_groups=mesh['tp'=8,'dp'=4] {'dp'}, dimensions={0}, use_global_device_ids=true | all-gather | bytes 163840 | tf_op jit(solution)/shard_map/all_gather | solution.py:101
  86.8 1.1 pad_maximum_fusion
  88.0 64.4 %reduce-scatter.7.cloned.1.call-done = f32[32,1024]{1,0:T(8,128)} async-done(((f32[256,1024]{1,0:T(8,128)}), f32[32,1024]{1,0:T(8,128)}) %reduce-scatter.7.cloned.1.call-update) | async-done | bytes 131088 | tf_op jit(solution)/shard_map/reduce_scatter | solution.py:103
  153.3 1.1 collective-permute-start.7
  154.4 5.6 %collective-permute-done.7 = bf16[32,512]{1,0:T(8,128)(2,1)S(1)} collective-permute-done((bf16[32,512]{1,0:T(8,128)(2,1)S(1)}, bf16[32,512]{1,0:T(8,128)(2,1)S(1)}, u32[]{:S(2)}, u32[]{:S(2)}) %collective-permute-start.7) | collective-permute-done | bytes 32800 | tf_op jit(solution)/shard_map/ppermute | solution.py:72
  159.9 6.6 %collective-permute-done.8 = bf16[32,512]{1,0:T(8,128)(2,1)S(1)} collective-permute-done((bf16[32,512]{1,0:T(8,128)(2,1)S(1)}, bf16[32,512]{1,0:T(8,128)(2,1)S(1)}, u32[]{:S(2)}, u32[]{:S(2)}) %collective-permute-start.8) | collective-permute-done | bytes 32800 | tf_op jit(solution)/shard_map/ppermute | solution.py:72
  166.5 6.7 %collective-permute-done.9 = bf16[32,512]{1,0:T(8,128)(2,1)S(1)} collective-permute-done((bf16[32,512]{1,0:T(8,128)(2,1)S(1)}, bf16[32,512]{1,0:T(8,128)(2,1)S(1)}, u32[]{:S(2)}, u32[]{:S(2)}) %collective-permute-start.9) | collective-permute-done | bytes 32800 | tf_op jit(solution)/shard_map/ppermute | solution.py:72
  173.3 6.6 %collective-permute-done.10 = bf16[32,512]{1,0:T(8,128)(2,1)S(1)} collective-permute-done((bf16[32,512]{1,0:T(8,128)(2,1)S(1)}, bf16[32,512]{1,0:T(8,128)(2,1)S(1)}, u32[]{:S(2)}, u32[]{:S(2)}) %collective-permute-start.10) | collective-permute-done | bytes 32800 | tf_op jit(solution)/shard_map/ppermute | solution.py:72
  179.9 6.6 %collective-permute-done.11 = bf16[32,512]{1,0:T(8,128)(2,1)S(1)} collective-permute-done((bf16[32,512]{1,0:T(8,128)(2,1)S(1)}, bf16[32,512]{1,0:T(8,128)(2,1)S(1)}, u32[]{:S(2)}, u32[]{:S(2)}) %collective-permute-start.11) | collective-permute-done | bytes 32800 | tf_op jit(solution)/shard_map/ppermute | solution.py:72
  186.5 6.6 %collective-permute-done.12 = bf16[32,512]{1,0:T(8,128)(2,1)S(1)} collective-permute-done((bf16[32,512]{1,0:T(8,128)(2,1)S(1)}, bf16[32,512]{1,0:T(8,128)(2,1)S(1)}, u32[]{:S(2)}, u32[]{:S(2)}) %collective-permute-start.12) | collective-permute-done | bytes 32800 | tf_op jit(solution)/shard_map/ppermute | solution.py:72
  193.1 6.6 %collective-permute-done.13 = bf16[32,512]{1,0:T(8,128)(2,1)S(1)} collective-permute-done((bf16[32,512]{1,0:T(8,128)(2,1)S(1)}, bf16[32,512]{1,0:T(8,128)(2,1)S(1)}, u32[]{:S(2)}, u32[]{:S(2)}) %collective-permute-start.13) | collective-permute-done | bytes 32800 | tf_op jit(solution)/shard_map/ppermute | solution.py:72
  199.8 2.0 fusion.10
  202.2 5.7 %all-reduce.1 = f32[256]{0:T(256)S(1)} all-reduce(f32[256]{0:T(256)S(1)} %fusion.6), channel_id=5, replica_groups=mesh['tp'=8,'dp'=4] {'dp'}, use_global_device_ids=true, to_apply=%region_5.7.clone | all-reduce | flops 256 | bytes 2048
  208.0 11.3 %reduce-scatter.9.cloned.1.call-done = f32[64,256]{1,0:T(8,128)} async-done(((f32[256,256]{1,0:T(8,128)}), f32[64,256]{1,0:T(8,128)}) %reduce-scatter.9.cloned.1.call-update) | async-done | bytes 65552 | tf_op jit(solution)/shard_map/reduce_scatter | solution.py:84
  220.3 1.0 fusion
  225.2 5.5 %all_gather.7 = bf16[256,256]{1,0:T(8,128)(2,1)S(1)} all-gather(bf16[64,256]{1,0:T(8,128)(2,1)S(1)} %fusion.73), channel_id=1, replica_groups=mesh['tp'=8,'dp'=4] {'dp'}, dimensions={0}, use_global_device_ids=true | all-gather | bytes 163840 | tf_op jit(solution)/shard_map/all_gather | solution.py:101
  231.3 1.1 pad_maximum_fusion.1
  232.9 1.6 copy.38
  234.4 62.3 %reduce-scatter.11.cloned.1.call-done = f32[32,1024]{1,0:T(8,128)} async-done(((f32[256,1024]{1,0:T(8,128)}), f32[32,1024]{1,0:T(8,128)}) %reduce-scatter.11.cloned.1.call-update) | async-done | bytes 131088 | tf_op jit(solution)/shard_map/reduce_scatter | solution.py:103
  296.7 1.5 fusion.93
  (110 shorter events, 17.4 us)
Async XLA Ops:
  7.2 21.5 %copy-start.17 = (f32[2,16]{1,0:T(2,128)S(1)}, f32[2,16]{1,0:T(2,128)}, u32[]{:S(2)}) copy-start(f32[2,16]{1,0:T(2,128)} %param.21) | copy-start | bytes 388
  7.2 67.7 %reduce-scatter.5.cloned.1.call-start = ((), (), s32[]{:S(2)}) async-start(), calls=%async_computation.4 | async-start | bytes 327680 | tf_op jit(solution)/shard_map/reduce_scatter | solution.py:84
  7.2 8.2 %collective-permute-start = (bf16[32,512]{1,0:T(8,128)(2,1)}, bf16[32,512]{1,0:T(8,128)(2,1)S(1)}, u32[]{:S(2)}, u32[]{:S(2)}) collective-permute-start(bf16[32,512]{1,0:T(8,128)(2,1)} %param.16), channel_id=1, source_target_pairs={{0,4},{4,8},{8,12},{12,16},{16,20},{20,24},{24,28},{28,0},{1,5},{5... | collective-permute-start | bytes 98312 | tf_op jit(solution)/shard_map/ppermute | solution.py:72
  15.4 6.6 %collective-permute-start.1 = (bf16[32,512]{1,0:T(8,128)(2,1)S(1)}, bf16[32,512]{1,0:T(8,128)(2,1)S(1)}, u32[]{:S(2)}, u32[]{:S(2)}) collective-permute-start(bf16[32,512]{1,0:T(8,128)(2,1)S(1)} %collective-permute-done), channel_id=1, source_target_pairs={{0,4},{4,8},{8,12},{12,16},{16,20},{20,24},{24,28},{28,0},{1,5},{5... | collective-permute-start | bytes 98312 | tf_op jit(solution)/shard_map/ppermute | solution.py:72
  22.0 6.6 %collective-permute-start.2 = (bf16[32,512]{1,0:T(8,128)(2,1)S(1)}, bf16[32,512]{1,0:T(8,128)(2,1)S(1)}, u32[]{:S(2)}, u32[]{:S(2)}) collective-permute-start(bf16[32,512]{1,0:T(8,128)(2,1)S(1)} %collective-permute-done.1), channel_id=1, source_target_pairs={{0,4},{4,8},{8,12},{12,16},{16,20},{20,24},{24,28},{28,0},{1,5},{5... | collective-permute-start | bytes 98312 | tf_op jit(solution)/shard_map/ppermute | solution.py:72
  22.0 13.2 %copy-start.13 = (f32[2,16,64]{2,1,0:T(8,128)S(1)}, f32[2,16,64]{2,1,0:T(8,128)}, u32[]{:S(2)}) copy-start(f32[2,16,64]{2,1,0:T(8,128)} %param.20) | copy-start | bytes 24580
  22.0 13.2 %copy-start.14 = (f32[2,16,64]{2,1,0:T(8,128)S(1)}, f32[2,16,64]{2,1,0:T(8,128)}, u32[]{:S(2)}) copy-start(f32[2,16,64]{2,1,0:T(8,128)} %param.19) | copy-start | bytes 24580
  22.0 34.2 %copy-start.18 = (bf16[2,512,256]{2,1,0:T(8,128)(2,1)S(1)}, bf16[2,512,256]{2,1,0:T(8,128)(2,1)}, u32[]{:S(2)}) copy-start(bf16[2,512,256]{2,1,0:T(8,128)(2,1)} %param.18) | copy-start | bytes 1572868
  28.6 6.6 %collective-permute-start.3 = (bf16[32,512]{1,0:T(8,128)(2,1)S(1)}, bf16[32,512]{1,0:T(8,128)(2,1)S(1)}, u32[]{:S(2)}, u32[]{:S(2)}) collective-permute-start(bf16[32,512]{1,0:T(8,128)(2,1)S(1)} %collective-permute-done.2), channel_id=1, source_target_pairs={{0,4},{4,8},{8,12},{12,16},{16,20},{20,24},{24,28},{28,0},{1,5},{5... | collective-permute-start | bytes 98312 | tf_op jit(solution)/shard_map/ppermute | solution.py:72
  35.2 7.0 %collective-permute-start.4 = (bf16[32,512]{1,0:T(8,128)(2,1)S(1)}, bf16[32,512]{1,0:T(8,128)(2,1)S(1)}, u32[]{:S(2)}, u32[]{:S(2)}) collective-permute-start(bf16[32,512]{1,0:T(8,128)(2,1)S(1)} %collective-permute-done.3), channel_id=1, source_target_pairs={{0,4},{4,8},{8,12},{12,16},{16,20},{20,24},{24,28},{28,0},{1,5},{5... | collective-permute-start | bytes 98312 | tf_op jit(solution)/shard_map/ppermute | solution.py:72
  35.4 13.4 %copy-start.15 = (f32[2,512]{1,0:T(2,128)S(1)}, f32[2,512]{1,0:T(2,128)}, u32[]{:S(2)}) copy-start(f32[2,512]{1,0:T(2,128)} %param.17) | copy-start | bytes 12292
  42.2 6.6 %collective-permute-start.5 = (bf16[32,512]{1,0:T(8,128)(2,1)S(1)}, bf16[32,512]{1,0:T(8,128)(2,1)S(1)}, u32[]{:S(2)}, u32[]{:S(2)}) collective-permute-start(bf16[32,512]{1,0:T(8,128)(2,1)S(1)} %collective-permute-done.4), channel_id=1, source_target_pairs={{0,4},{4,8},{8,12},{12,16},{16,20},{20,24},{24,28},{28,0},{1,5},{5... | collective-permute-start | bytes 98312 | tf_op jit(solution)/shard_map/ppermute | solution.py:72
  48.8 6.6 %collective-permute-start.6 = (bf16[32,512]{1,0:T(8,128)(2,1)S(1)}, bf16[32,512]{1,0:T(8,128)(2,1)S(1)}, u32[]{:S(2)}, u32[]{:S(2)}) collective-permute-start(bf16[32,512]{1,0:T(8,128)(2,1)S(1)} %collective-permute-done.5), channel_id=1, source_target_pairs={{0,4},{4,8},{8,12},{12,16},{16,20},{20,24},{24,28},{28,0},{1,5},{5... | collective-permute-start | bytes 98312 | tf_op jit(solution)/shard_map/ppermute | solution.py:72
  57.4 95.0 %reduce-scatter.7.cloned.1.call-start = ((), (), s32[]{:S(2)}) async-start(), calls=%async_computation.5 | async-start | bytes 1179648 | tf_op jit(solution)/shard_map/reduce_scatter | solution.py:103
  60.2 15.6 %copy-start = (f32[2,16,64,16]{2,3,1,0:T(8,128)S(1)}, f32[2,16,64,16]{2,3,1,0:T(8,128)}, u32[]{:S(2)}) copy-start(f32[2,16,64,16]{2,3,1,0:T(8,128)} %param.23) | copy-start | bytes 393220
  60.2 15.6 %copy-start.1 = (f32[2,16,64,16]{2,3,1,0:T(8,128)S(1)}, f32[2,16,64,16]{2,3,1,0:T(8,128)}, u32[]{:S(2)}) copy-start(f32[2,16,64,16]{2,3,1,0:T(8,128)} %param.22) | copy-start | bytes 393220
  76.9 1.1 copy-start.10
  78.0 1.0 copy-start.6
  78.9 7.5 %copy-start.2 = (bf16[2,256,512]{2,1,0:T(8,128)(2,1)S(1)}, bf16[2,256,512]{2,1,0:T(8,128)(2,1)}, u32[]{:S(2)}) copy-start(bf16[2,256,512]{2,1,0:T(8,128)(2,1)} %param.28) | copy-start | bytes 1572868
  80.8 5.8 %copy-start.4 = (bf16[2,256,512]{2,1,0:T(8,128)(2,1)S(1)}, bf16[2,256,512]{2,1,0:T(8,128)(2,1)}, u32[]{:S(2)}) copy-start(bf16[2,256,512]{2,1,0:T(8,128)(2,1)} %param.27) | copy-start | bytes 1572868
  87.9 131.3 %reduce-scatter.9.cloned.1.call-start = ((), (), s32[]{:S(2)}) async-start(), calls=%async_computation.6 | async-start | bytes 327680 | tf_op jit(solution)/shard_map/reduce_scatter | solution.py:84
  153.3 6.7 %collective-permute-start.7 = (bf16[32,512]{1,0:T(8,128)(2,1)S(1)}, bf16[32,512]{1,0:T(8,128)(2,1)S(1)}, u32[]{:S(2)}, u32[]{:S(2)}) collective-permute-start(bf16[32,512]{1,0:T(8,128)(2,1)S(1)} %fusion.92), channel_id=1, source_target_pairs={{0,4},{4,8},{8,12},{12,16},{16,20},{20,24},{24,28},{28,0},{1,5},{5... | collective-permute-start | bytes 98312 | tf_op jit(solution)/shard_map/ppermute | solution.py:72
  159.9 6.6 %collective-permute-start.8 = (bf16[32,512]{1,0:T(8,128)(2,1)S(1)}, bf16[32,512]{1,0:T(8,128)(2,1)S(1)}, u32[]{:S(2)}, u32[]{:S(2)}) collective-permute-start(bf16[32,512]{1,0:T(8,128)(2,1)S(1)} %collective-permute-done.7), channel_id=1, source_target_pairs={{0,4},{4,8},{8,12},{12,16},{16,20},{20,24},{24,28},{28,0},{1,5},{5... | collective-permute-start | bytes 98312 | tf_op jit(solution)/shard_map/ppermute | solution.py:72
  166.5 6.7 %collective-permute-start.9 = (bf16[32,512]{1,0:T(8,128)(2,1)S(1)}, bf16[32,512]{1,0:T(8,128)(2,1)S(1)}, u32[]{:S(2)}, u32[]{:S(2)}) collective-permute-start(bf16[32,512]{1,0:T(8,128)(2,1)S(1)} %collective-permute-done.8), channel_id=1, source_target_pairs={{0,4},{4,8},{8,12},{12,16},{16,20},{20,24},{24,28},{28,0},{1,5},{5... | collective-permute-start | bytes 98312 | tf_op jit(solution)/shard_map/ppermute | solution.py:72
  173.3 6.6 %collective-permute-start.10 = (bf16[32,512]{1,0:T(8,128)(2,1)S(1)}, bf16[32,512]{1,0:T(8,128)(2,1)S(1)}, u32[]{:S(2)}, u32[]{:S(2)}) collective-permute-start(bf16[32,512]{1,0:T(8,128)(2,1)S(1)} %collective-permute-done.9), channel_id=1, source_target_pairs={{0,4},{4,8},{8,12},{12,16},{16,20},{20,24},{24,28},{28,0},{1,5},{5... | collective-permute-start | bytes 98312 | tf_op jit(solution)/shard_map/ppermute | solution.py:72
  179.9 6.6 %collective-permute-start.11 = (bf16[32,512]{1,0:T(8,128)(2,1)S(1)}, bf16[32,512]{1,0:T(8,128)(2,1)S(1)}, u32[]{:S(2)}, u32[]{:S(2)}) collective-permute-start(bf16[32,512]{1,0:T(8,128)(2,1)S(1)} %collective-permute-done.10), channel_id=1, source_target_pairs={{0,4},{4,8},{8,12},{12,16},{16,20},{20,24},{24,28},{28,0},{1,5},{5... | collective-permute-start | bytes 98312 | tf_op jit(solution)/shard_map/ppermute | solution.py:72
  186.5 6.6 %collective-permute-start.12 = (bf16[32,512]{1,0:T(8,128)(2,1)S(1)}, bf16[32,512]{1,0:T(8,128)(2,1)S(1)}, u32[]{:S(2)}, u32[]{:S(2)}) collective-permute-start(bf16[32,512]{1,0:T(8,128)(2,1)S(1)} %collective-permute-done.11), channel_id=1, source_target_pairs={{0,4},{4,8},{8,12},{12,16},{16,20},{20,24},{24,28},{28,0},{1,5},{5... | collective-permute-start | bytes 98312 | tf_op jit(solution)/shard_map/ppermute | solution.py:72
  193.1 6.6 %collective-permute-start.13 = (bf16[32,512]{1,0:T(8,128)(2,1)S(1)}, bf16[32,512]{1,0:T(8,128)(2,1)S(1)}, u32[]{:S(2)}, u32[]{:S(2)}) collective-permute-start(bf16[32,512]{1,0:T(8,128)(2,1)S(1)} %collective-permute-done.12), channel_id=1, source_target_pairs={{0,4},{4,8},{8,12},{12,16},{16,20},{20,24},{24,28},{28,0},{1,5},{5... | collective-permute-start | bytes 98312 | tf_op jit(solution)/shard_map/ppermute | solution.py:72
  201.8 94.9 %reduce-scatter.11.cloned.1.call-start = ((), (), s32[]{:S(2)}) async-start(), calls=%async_computation.7 | async-start | bytes 1179648 | tf_op jit(solution)/shard_map/reduce_scatter | solution.py:103
  221.3 1.1 copy-start.11
  223.3 7.4 %copy-start.3 = (bf16[2,256,512]{2,1,0:T(8,128)(2,1)S(1)}, bf16[2,256,512]{2,1,0:T(8,128)(2,1)}, u32[]{:S(2)}) copy-start(bf16[2,256,512]{2,1,0:T(8,128)(2,1)} %param.28) | copy-start | bytes 1572868
  225.2 5.8 %copy-start.5 = (bf16[2,256,512]{2,1,0:T(8,128)(2,1)S(1)}, bf16[2,256,512]{2,1,0:T(8,128)(2,1)}, u32[]{:S(2)}) copy-start(bf16[2,256,512]{2,1,0:T(8,128)(2,1)} %param.27) | copy-start | bytes 1572868
  (6 other events, 4.8 us)
Sparse Core Ops, SparseCore 0:
  57.5 17.3 reduce-scatter.4
  88.1 64.2 reduce-scatter.6
  202.0 17.2 reduce-scatter.8
  232.5 64.1 reduce-scatter.10
